TPU v7x, 32 devices: a whole 2x2x4 slice. The times are simulated.
32 devices in a mesh: sp: 8 (over z, y), tp: 4 (over x, core).
Axes of the slice: x: 2, y: 2, z: 4, core: 2. Of those that a mesh axis runs over, the one named last changes fastest.
Arguments:
- queries: bfloat16 [8192, 512], P('sp', 'tp'), may hold values from -6 to 6
- keys: bfloat16 [8192, 512], P('sp', 'tp'), may hold values from -6 to 6
- values: bfloat16 [8192, 1024], P('sp', 'tp'), may hold values from -6 to 6
- out_gate: bfloat16 [8192, 1024], P('sp', 'tp'), may hold values from -6 to 6
- decay_logit: float32 [2, 8192, 512], P(None, 'sp', 'tp'), may hold values from -8 to 16
- head_gain: float32 [1024], P('tp'), may hold values from 0.1 to 1.9
- out_weight: bfloat16 [1024, 2048], replicated, may hold values from -0.1875 to 0.1875
- stream: bfloat16 [8192, 2048], P(('sp', 'tp')), may hold values from -6 to 6
- mlp_gain: float32 [2048], replicated, may hold values from 0.1 to 1.9
- up_weight: bfloat16 [2048, 8192], P('sp', 'tp'), may hold values from -0.125 to 0.125
- down_weight: bfloat16 [8192, 2048], P('tp', 'sp'), may hold values from -0.0625 to 0.0625
Outputs:
- output: bfloat16 [8192, 2048], P(('sp', 'tp'))
All inputs are finite; a program needn't handle non-finite values.
Results may differ from a plain program's by a relative error of at most 0.018.
Values may be sent and summed in bfloat16 or wider, within the bound.
A program may use at most 128 MiB of HBM per device.

v0:
```python
import jax
import jax.numpy as jnp
from jax import lax
from jax.sharding import PartitionSpec as P

HEAD_K = 64
HEAD_V = 128
BLOCK = 64


gate_temper = 16.0
norm_eps = 1e-06
highest = lax.Precision.HIGHEST


def carried_in(x, axis, combine, identity, reverse):
    count, position = (lax.axis_size(axis), lax.axis_index(axis))
    everything = jax.tree.map(
        lambda part, kind: lax.all_gather(part.astype(kind), axis), x, (jnp.bfloat16, jnp.bfloat16)
    )
    start = jax.tree.map(
        lambda part, zero: jnp.broadcast_to(jnp.asarray(zero, part.dtype), part.shape), x, identity
    )

    def hop(k, before):
        at = count - 1 - k if reverse else k
        reached = at > position if reverse else at < position
        new = combine(
            before, jax.tree.map(lambda part, own: part[at].astype(own.dtype), everything, x)
        )
        return jax.tree.map(lambda a, b: jnp.where(reached, a, b), new, before)

    return lax.fori_loop(0, count, hop, start)


def blockwise(query_rows, key_rows, value_rows, log_decay):
    length, number_of_heads, key_size = query_rows.shape
    value_size = value_rows.shape[2]
    block_count = length // BLOCK
    query_blk = query_rows.reshape(block_count, BLOCK, number_of_heads, key_size)
    key_blk = key_rows.reshape(block_count, BLOCK, number_of_heads, key_size)
    value_blk = value_rows.reshape(block_count, BLOCK, number_of_heads, value_size)
    within = jnp.cumsum(log_decay.reshape(block_count, BLOCK, number_of_heads, key_size), axis=1)
    block_end = within[:, -1]
    query_dec = query_blk * jnp.exp(within)
    key_inv = key_blk * jnp.exp(-within)
    key_end = key_blk * jnp.exp(block_end[:, None] - within)
    lower_mask = jnp.tril(jnp.ones((BLOCK, BLOCK), dtype=bool))
    scores = jnp.einsum("nihd,njhd->nhij", query_dec, key_inv, precision=highest)
    scores = jnp.where(lower_mask, scores, jnp.float32(0.0))
    intra_out = jnp.einsum("nhij,njhe->nihe", scores, value_blk, precision=highest)
    increments = jnp.einsum("njhd,njhe->nhde", key_end, value_blk, precision=highest)

    def advance(carried, inputs):
        decay_end, increment = inputs
        return (decay_end[..., None] * carried + increment, carried)

    start_state = jnp.zeros((number_of_heads, key_size, value_size), jnp.float32)
    state_end, state_in = lax.scan(advance, start_state, (jnp.exp(block_end), increments))
    inter_out = jnp.einsum("nihd,nhde->nihe", query_dec, state_in, precision=highest)
    return ((intra_out + inter_out).reshape(length, number_of_heads, value_size), state_end)


def summarize(query_rows, key_rows, value_rows, log_decay):
    local_out, state_end = blockwise(query_rows, key_rows, value_rows, log_decay)
    running = jnp.cumsum(log_decay, axis=0)
    carry_query = query_rows * jnp.exp(running)
    return (local_out, carry_query, jnp.exp(running[-1]), state_end)


def chain_states(earlier, later_one):
    return (earlier[0] * later_one[0], later_one[0][..., None] * earlier[1] + later_one[1])


def rms_scale(rows_in, gain_vec):
    widened = rows_in.astype(jnp.float32)
    inv_rms = lax.rsqrt(jnp.mean(widened * widened, axis=-1, keepdims=True) + norm_eps)
    return (widened * inv_rms * gain_vec).astype(jnp.bfloat16)


def local(
    queries,
    keys,
    values,
    out_gate,
    decay_logit,
    head_gain,
    out_weight,
    stream,
    mlp_gain,
    up_weight,
    down_weight,
):
    length = queries.shape[0]
    number_of_heads = queries.shape[1] // HEAD_K
    query_heads = queries.astype(jnp.float32).reshape(length, number_of_heads, HEAD_K) * HEAD_K ** (
        -0.5
    )
    key_heads = keys.astype(jnp.float32).reshape(length, number_of_heads, HEAD_K)
    value_heads = values.astype(jnp.float32).reshape(length, number_of_heads, HEAD_V)
    log_decay = (jax.nn.log_sigmoid(decay_logit) / gate_temper).reshape(
        2, length, number_of_heads, HEAD_K
    )
    fwd_local, fwd_query, fwd_decay, fwd_state = summarize(
        query_heads, key_heads, value_heads, log_decay[0]
    )
    bwd_local, bwd_query, bwd_decay, bwd_state = summarize(
        jnp.flip(query_heads, 0),
        jnp.flip(key_heads, 0),
        jnp.flip(value_heads, 0),
        jnp.flip(log_decay[1], 0),
    )
    identity = (jnp.ones_like(fwd_decay), jnp.zeros_like(fwd_state))
    fwd_in = carried_in((fwd_decay, fwd_state), "sp", chain_states, identity, False)[1]
    bwd_in = carried_in((bwd_decay, bwd_state), "sp", chain_states, identity, True)[1]
    fwd_out = fwd_local + jnp.einsum("lhd,hde->lhe", fwd_query, fwd_in, precision=highest)
    bwd_out = bwd_local + jnp.einsum("lhd,hde->lhe", bwd_query, bwd_in, precision=highest)
    attended = fwd_out + jnp.flip(bwd_out, 0)
    inv_rms = lax.rsqrt(jnp.mean(attended * attended, axis=-1, keepdims=True) + norm_eps)
    normed_heads = (attended * inv_rms * head_gain.reshape(number_of_heads, HEAD_V)).reshape(
        length, number_of_heads * HEAD_V
    )
    gated_rows = (normed_heads * jax.nn.silu(out_gate.astype(jnp.float32))).astype(jnp.bfloat16)
    up_full, down_full = (
        lax.all_gather(up_weight, "sp", axis=0, tiled=True),
        lax.all_gather(down_weight, "sp", axis=1, tiled=True),
    )
    tp_count = lax.axis_size("tp")
    own_rows = length // tp_count
    tp_index = lax.axis_index("tp")
    col_width = gated_rows.shape[1]
    weight_part = lax.dynamic_slice_in_dim(out_weight, tp_index * col_width, col_width, 0)
    partial_value = jnp.dot(gated_rows, weight_part, preferred_element_type=jnp.float32)
    placed = lax.dynamic_update_slice_in_dim(
        jnp.zeros_like(partial_value), stream.astype(jnp.float32), tp_index * own_rows, 0
    )
    summed = lax.psum((partial_value + placed).astype(jnp.bfloat16), "tp")
    hidden = jnp.square(
        jax.nn.relu(
            jnp.dot(rms_scale(summed, mlp_gain), up_full, preferred_element_type=jnp.float32)
        )
    ).astype(jnp.bfloat16)
    residual = lax.dynamic_slice_in_dim(summed, tp_index * own_rows, own_rows, 0)
    mlp_sum = lax.psum_scatter(
        jnp.dot(hidden, down_full, preferred_element_type=jnp.float32).astype(jnp.bfloat16),
        "tp",
        scatter_dimension=0,
        tiled=True,
    ).astype(jnp.float32)
    return (residual.astype(jnp.float32) + mlp_sum).astype(jnp.bfloat16)


def solution(mesh):
    in_specs = (
        P("sp", "tp"),
        P("sp", "tp"),
        P("sp", "tp"),
        P("sp", "tp"),
        P(None, "sp", "tp"),
        P("tp"),
        P(),
        P(("sp", "tp"), None),
        P(),
        P("sp", "tp"),
        P("tp", "sp"),
    )
    out_specs = P(("sp", "tp"), None)
    return jax.shard_map(local, mesh=mesh, in_specs=in_specs, out_specs=out_specs, check_vma=False)
```

profile of v0, /device:TPU:0, one launch (start us, length us, event | category | flops | bytes accessed | tf_op | source)
XLA Modules:
  0.0 695.0 jit_solution(3146252523181368258)
XLA Ops:
  7.4 1.6 copy.108
  9.6 1.0 slice_bitcast_fusion.2
  12.3 13.2 %fusion.61 = f32[16,64,2,64]{3,0,1,2:T(8,128)S(1)} fusion(f32[16,64,2,64]{3,0,1,2:T(8,128)S(1)} %copy.128), kind=kOutput, calls=%fused_computation.101 | output fusion | flops 8257536 | bytes 1048576 | tf_op jit(solution)/shard_map/jit(cumsum)/reduce_window_sum | solution.py:43
  28.1 1.3 reshape_reshape.6
  29.4 2.0 copy.133
  31.4 1.2 reshape_reshape.7
  33.6 13.2 %fusion.60 = f32[16,64,2,64]{3,0,1,2:T(8,128)S(1)} fusion(f32[16,64,2,64]{3,0,1,2:T(8,128)S(1)} %copy.109), kind=kOutput, calls=%fused_computation.100 | output fusion | flops 8257536 | bytes 1048576 | tf_op jit(solution)/shard_map/jit(cumsum)/reduce_window_sum | solution.py:43
  50.4 1.6 copy.129
  52.1 3.8 rev.19
  56.1 1.6 copy.130
  57.7 6.8 rev.20
  64.9 2.3 exponential_multiply_fusion
  67.2 2.5 convolution_select_fusion
  69.7 2.1 convolution_bitcast_fusion.3
  71.8 3.1 fusion.28
  75.0 37.2 %while.58 = (s32[]{:T(128)}, f32[2,64,128]{2,1,0:T(8,128)S(1)}, f32[16,2,64,128]{3,2,1,0:T(8,128)S(1)}, f32[16,2,64]{2,0,1:T(8,128)}, f32[16,2,64,128]{3,2,1,0:T(8,128)}, /*index=5*/s32[]{:T(128)}, s32[]{:T(128)}) while((s32[]{:T(128)}, f32[2,64,128]{2,1,0:T(8,128)S(1)}, f32[16,2,64,128]{3,2,1,0:T(8,128)S(1)}, ...), condition=%wide.region_9.10_spmd.clone, body=%wide.region_8.9_spmd.clone.sunk | while | flops 65539 | bytes 329316 | solution.py:59
  75.7 0.9 bitcast_add_fusion.5
  77.4 0.9 bitcast_add_fusion.5
  79.1 0.9 bitcast_add_fusion.5
  80.8 0.9 bitcast_add_fusion.5
  82.5 0.9 bitcast_add_fusion.5
  84.2 0.9 bitcast_add_fusion.5
  85.8 0.9 bitcast_add_fusion.5
  87.5 0.9 bitcast_add_fusion.5
  89.2 0.9 bitcast_add_fusion.5
  90.9 0.9 bitcast_add_fusion.5
  92.6 0.9 bitcast_add_fusion.5
  94.2 0.9 bitcast_add_fusion.5
  95.9 0.9 bitcast_add_fusion.5
  112.2 2.7 fusion.17
  115.1 1.3 copy.147
  116.4 34.5 %all-gather.1 = bf16[16,64,128]{2,1,0:T(8,128)(2,1)} all-gather(bf16[2,64,128]{2,1,0:T(8,128)(2,1)S(1)} %convert_element_type.113), channel_id=3, replica_groups=mesh['sp'=8,'tp'=4] {'sp'}, dimensions={0}, use_global_device_ids=true | all-gather | bytes 294912 | tf_op jit(solution)/shard_map/all_gather | solution.py:19
  150.9 1.1 copy.152
  152.1 36.0 %reduce-window.16 = f32[64,2,8,128]{3,2,1,0:T(8,128)S(1)} reduce-window(f32[64,2,8,128]{3,2,1,0:T(8,128)S(1)} %copy.142, f32[]{:T(128)} %constant.125.clone.1), window={size=1x1x1x128 pad=0_0x0_0x0_0x127_0}, to_apply=%region_10.11 | reduce-window | flops 16646144 | bytes 1048580 | tf_op jit(solution)/shard_map/reduce-window.2
  189.3 1.0 broadcast_add_fusion
  191.5 0.9 copy.146
  192.5 20.5 %all_gather.29 = bf16[8,2,64]{2,1,0:T(2,128)(2,1)S(1)} all-gather(bf16[1,2,64]{2,1,0:T(2,128)(2,1)S(1)} %exponential_convert_fusion), channel_id=1, replica_groups=mesh['sp'=8,'tp'=4] {'sp'}, dimensions={0}, use_global_device_ids=true | all-gather | bytes 2304 | tf_op jit(solution)/shard_map/all_gather | solution.py:19
  213.0 7.2 %while.59 = (s32[]{:T(128)}, f32[2,64,128]{2,1,0:T(8,128)S(1)}, s32[]{:T(128)}, bf16[8,2,64]{2,1,0:T(2,128)(2,1)S(1)}, bf16[8,2,64,128]{3,2,1,0:T(8,128)(2,1)}, ...) while((s32[]{:T(128)}, f32[2,64,128]{2,1,0:T(8,128)S(1)}, s32[]{:T(128)}, ...), condition=%wide.region_13.14_spmd.clone, body=%wide.region_12.13_spmd.clone.sunk | while | flops 82056 | bytes 165287 | solution.py:33
  220.2 3.3 fusion.21
  223.5 9.3 %rev.21 = f32[1024,2,128]{0,2,1:T(8,128)} reverse(f32[1024,2,128]{0,2,1:T(8,128)} %fusion.21), dimensions={0} | reverse | bytes 2097152 | tf_op jit(solution)/shard_map/jit(_flip)/rev | solution.py:118
  232.9 1.3 mul.163
  234.2 1.6 copy.110
  235.8 2.8 copy.112
  238.6 2.0 exponential_multiply_fusion.3
  240.6 2.5 convolution_select_fusion.1
  243.1 1.6 convolution_bitcast_fusion.5
  244.7 1.2 fusion.31
  246.1 13.5 %while.56 = (s32[]{:T(128)}, f32[2,64,128]{2,1,0:T(8,128)S(1)}, f32[16,2,64,128]{3,2,1,0:T(8,128)S(1)}, f32[16,2,64]{2,0,1:T(8,128)}, f32[16,2,64,128]{3,2,1,0:T(8,128)S(1)}, /*index=5*/s32[]{:T(128)}, s32[]{:T(128)}) while((s32[]{:T(128)}, f32[2,64,128]{2,1,0:T(8,128)S(1)}, f32[16,2,64,128]{3,2,1,0:T(8,128)S(1)}, ...), condition=%wide.region_2.3_spmd.clone, body=%wide.region_1.2_spmd.clone.sunk | while | flops 65539 | bytes 329316 | solution.py:59
  259.6 2.8 fusion.18
  262.9 32.8 %all-gather = bf16[16,64,128]{2,1,0:T(8,128)(2,1)} all-gather(bf16[2,64,128]{2,1,0:T(8,128)(2,1)S(1)} %convert_element_type.111), channel_id=2, replica_groups=mesh['sp'=8,'tp'=4] {'sp'}, dimensions={0}, use_global_device_ids=true | all-gather | bytes 294912 | tf_op jit(solution)/shard_map/all_gather | solution.py:19
  295.6 1.1 copy.151
  296.8 36.0 %reduce-window.14 = f32[64,2,8,128]{3,2,1,0:T(8,128)S(1)} reduce-window(f32[64,2,8,128]{3,2,1,0:T(8,128)S(1)} %copy.122, f32[]{:T(128)} %constant.125.clone.1), window={size=1x1x1x128 pad=0_0x0_0x0_0x127_0}, to_apply=%region_3.4 | reduce-window | flops 16646144 | bytes 1048580 | tf_op jit(solution)/shard_map/reduce-window
  334.3 16.3 %all_gather.26 = bf16[8,2,64]{2,1,0:T(2,128)(2,1)S(1)} all-gather(bf16[1,2,64]{2,1,0:T(2,128)(2,1)S(1)} %exponential_convert_fusion.1), channel_id=1, replica_groups=mesh['sp'=8,'tp'=4] {'sp'}, dimensions={0}, use_global_device_ids=true | all-gather | bytes 2304 | tf_op jit(solution)/shard_map/all_gather | solution.py:19
  350.6 7.2 %while.57 = (s32[]{:T(128)}, f32[2,64,128]{2,1,0:T(8,128)S(1)}, s32[]{:T(128)}, bf16[8,2,64]{2,1,0:T(2,128)(2,1)S(1)}, bf16[8,2,64,128]{3,2,1,0:T(8,128)(2,1)}, /*index=5*/s32[]{:T(128)}, s32[]{:T(128)}) while((s32[]{:T(128)}, f32[2,64,128]{2,1,0:T(8,128)S(1)}, s32[]{:T(128)}, bf16[8,2,64]{2,1,0:T(2,128)(2,1)S(1)}, ...), condition=%wide.region_6.7_spmd.clone, body=%wide.region_5.6_spmd.clone.sunk | while | flops 82052 | bytes 165225 | solution.py:33
  357.7 1.2 multiply_reduce_fusion
  359.6 2.7 fusion.34
  362.7 2.6 convert_element_type.117
  366.6 83.1 %all-reduce.2.cloned.1.call-done = bf16[1024,2048]{1,0:T(8,128)(2,1)} async-done(((bf16[1024,2048]{1,0:T(8,128)(2,1)}), bf16[1024,2048]{1,0:T(8,128)(2,1)}) %all-reduce.2.cloned.1.call-update) | async-done | bytes 4194320 | tf_op jit(solution)/shard_map/psum | solution.py:137
  449.7 3.1 fusion.2
  452.7 38.1 %all-gather.5.cloned.1.call-done = bf16[2048,2048]{1,0:T(8,128)(2,1)} async-done(((bf16[256,2048]{1,0:T(8,128)(2,1)}), bf16[2048,2048]{1,0:T(8,128)(2,1)}) %all-gather.5.cloned.1.call-update) | async-done | bytes 8388624 | tf_op jit(solution)/shard_map/all_gather | solution.py:125
  490.8 124.9 %all-gather.7.cloned.1.call-done = bf16[2048,2048]{1,0:T(8,128)(2,1)} async-done(((bf16[2048,256]{1,0:T(8,128)(2,1)}), bf16[2048,2048]{1,0:T(8,128)(2,1)}) %all-gather.7.cloned.1.call-update) | async-done | bytes 8388624 | tf_op jit(solution)/shard_map/all_gather | solution.py:126
  615.7 25.6 %fusion.14 = bf16[1024,2048]{1,0:T(8,128)(2,1)} fusion(bf16[2048,2048]{1,0:T(8,128)(2,1)} %all-gather.7.cloned.1.call-done, bf16[2048,2048]{1,0:T(8,128)(2,1)} %all-gather.5.cloned.1.call-done, bf16[1024,2048]{1,0:T(8,128)(2,1)} %all-reduce.2.cloned.1.call-done, f32[2048]{0:T(1024)S(1)} %copy-done.12, f32[1024]{0:T(1024)S(1)} %add_rsqrt_fusion.1), kind=kOutput, calls=%fused_computation.22 | convolution fusion | flops 17196646400 | bytes 25178112 | tf_op jit(solution)/shard_map/dot_general | solution.py:145
  641.4 42.9 %reduce-scatter.2.cloned.1.call-done = bf16[256,2048]{1,0:T(8,128)(2,1)} async-done(((bf16[1024,2048]{1,0:T(8,128)(2,1)}), bf16[256,2048]{1,0:T(8,128)(2,1)}) %reduce-scatter.2.cloned.1.call-update) | async-done | bytes 1048592 | tf_op jit(solution)/shard_map/reduce_scatter | solution.py:144
  684.3 2.9 add_convert_fusion
  (207 shorter events, 58.0 us)
Async XLA Ops:
  7.4 19.8 %copy-start.8 = (bf16[1024,128]{1,0:T(8,128)(2,1)S(1)}, bf16[1024,128]{1,0:T(8,128)(2,1)}, u32[]{:S(2)}) copy-start(bf16[1024,128]{1,0:T(8,128)(2,1)} %param.20) | copy-start | bytes 786436
  7.4 442.3 %all-reduce.2.cloned.1.call-start = ((), (), s32[]{:S(2)}) async-start(), calls=%async_computation.1 | async-start | bytes 8388608 | tf_op jit(solution)/shard_map/psum | solution.py:137
  11.3 18.0 %copy-start = (f32[1024,2,64]{0,2,1:T(8,128)}, f32[1024,2,64]{0,2,1:T(8,128)S(1)}, u32[]{:S(2)}) copy-start(f32[1024,2,64]{0,2,1:T(8,128)S(1)} %rev.18) | copy-start | bytes 1572868
  25.5 1.0 copy-start.3
  25.5 22.8 %copy-start.9 = (bf16[1024,128]{1,0:T(8,128)(2,1)S(1)}, bf16[1024,128]{1,0:T(8,128)(2,1)}, u32[]{:S(2)}) copy-start(bf16[1024,128]{1,0:T(8,128)(2,1)} %param.19) | copy-start | bytes 786436
  46.7 1.0 copy-start.1
  115.0 98.0 %copy-start.6 = (f32[2,64,128]{2,1,0:T(8,128)S(1)}, f32[2,64,128]{2,1,0:T(8,128)}, u32[]{:S(2)}) copy-start(f32[2,64,128]{2,1,0:T(8,128)} %custom-call.3) | copy-start | bytes 196612
  188.1 50.5 %copy-start.2 = (f32[16,64,2,64]{3,0,1,2:T(8,128)S(1)}, f32[16,64,2,64]{3,0,1,2:T(8,128)}, u32[]{:S(2)}) copy-start(f32[16,64,2,64]{3,0,1,2:T(8,128)} %copy-done.1) | copy-start | bytes 1572868
  191.5 47.1 %copy-start.10 = (f32[16,2,64]{2,0,1:T(8,128)S(1)}, f32[16,2,64]{2,0,1:T(8,128)}, u32[]{:S(2)}) copy-start(f32[16,2,64]{2,0,1:T(8,128)} %slice_bitcast_fusion.1) | copy-start | bytes 24580
  259.6 91.0 %copy-start.5 = (f32[2,64,128]{2,1,0:T(8,128)S(1)}, f32[2,64,128]{2,1,0:T(8,128)}, u32[]{:S(2)}) copy-start(f32[2,64,128]{2,1,0:T(8,128)} %custom-call.1) | copy-start | bytes 196612
  259.6 98.2 %copy-start.4 = (f32[1024,2,128]{0,2,1:T(8,128)S(1)}, f32[1024,2,128]{0,2,1:T(8,128)}, u32[]{:S(2)}) copy-start(f32[1024,2,128]{0,2,1:T(8,128)} %rev.21) | copy-start | bytes 3145732
  262.5 96.5 %copy-start.11 = (f32[256]{0:T(256)S(1)}, f32[256]{0:T(256)}, u32[]{:S(2)}) copy-start(f32[256]{0:T(256)} %param.24) | copy-start | bytes 3076
  359.0 3.3 copy-start.7
  365.3 250.4 %copy-start.12 = (f32[2048]{0:T(1024)S(1)}, f32[2048]{0:T(1024)}, u32[]{:S(2)}) copy-start(f32[2048]{0:T(1024)} %param.27) | copy-start | bytes 24580
  365.4 125.5 %all-gather.5.cloned.1.call-start = ((), (), s32[]{:S(2)}) async-start(), calls=%async_computation.2 | async-start | bytes 9437184 | tf_op jit(solution)/shard_map/all_gather | solution.py:125
  365.9 249.7 %all-gather.7.cloned.1.call-start = ((), (), s32[]{:S(2)}) async-start(), calls=%async_computation.3 | async-start | bytes 9437184 | tf_op jit(solution)/shard_map/all_gather | solution.py:126
  366.5 317.8 %reduce-scatter.2.cloned.1.call-start = ((), (), s32[]{:S(2)}) async-start(), calls=%async_computation.4 | async-start | bytes 5242880 | tf_op jit(solution)/shard_map/reduce_scatter | solution.py:144
Sparse Core Ops, SparseCore 0:
  365.5 84.1 all-reduce.1
  641.5 42.7 reduce-scatter.1
Sparse Core Ops, SparseCore 1:
  368.0 122.8 all-gather.4
  492.7 122.9 all-gather.6
where the time goes:
time: 705 us; the launch traced here: 695 us
  waiting for transfers between devices  290 us (41%)
  other arithmetic  146 us (21%)
  blocking collectives  104 us (15%)
  local copies, waits for them, and re-layouts  75.6 us (11%)
  matrix products  51.5 us (7%)
  between operations  15.7 us (2%)
  loops' own time  12 us (2%)
    all_gather x1, waiting for transfers between devices, local(): lax.all_gather(down_weight, 'sp', axis=1, tiled=True)  125 us
    all_gather x4, blocking collectives, carried_in(): lax.all_gather(part.astype(kind), axis)  104 us
    psum x1, waiting for transfers between devices, local(): summed = lax.psum((partial_value + placed).astype(jnp.bfloat16), 'tp')  83.1 us
    another operation x6, other arithmetic  73.3 us
    reduce_scatter x1, waiting for transfers between devices, local(): lax.psum_scatter(jnp.dot(hidden, down_full, preferred_element_type=jnp.fl...  42.9 us
    all_gather x1, waiting for transfers between devices, local(): lax.all_gather(up_weight, 'sp', axis=0, tiled=True)  38.1 us
    another operation x2, other arithmetic, blockwise(): jnp.cumsum(log_decay.reshape(block_count, BLOCK, number_of_heads, key_siz...  26.3 us
    dot_general x1, matrix products, local(): jnp.dot(hidden, down_full, preferred_element_type=jnp.float32)  25.6 us
  transfers between devices with their start and end apart: 4, of which 4 were waited for; matrix products, arithmetic and copies ran while one was open for 0% of the time, Pallas kernels for 0%

commit v1 on v0

v1 whole, which is shorter than its diff:
```python
import functools
import jax
import jax.numpy as jnp
from jax import lax
from jax.experimental import pallas as pl
from jax.experimental.pallas import tpu as pltpu
from jax.sharding import PartitionSpec as P

HEAD_K = 64
HEAD_V = 128
CHUNK = 128
gate_temper = 16.0
norm_eps = 1e-06
MESH = pl.DeviceIdType.MESH
f32 = jnp.float32
bf16 = jnp.bfloat16


def dot(a, b):
    return jnp.dot(a, b, preferred_element_type=f32)


def dot_t0(a, b):
    return lax.dot_general(a, b, (((0,), (0,)), ((), ())), preferred_element_type=f32)


def dot_t1(a, b):
    return lax.dot_general(a, b, (((1,), (1,)), ((), ())), preferred_element_type=f32)


def split_hi_lo(x):
    hi = x.astype(bf16)
    return hi, (x - hi.astype(f32)).astype(bf16)


def attention_kernel(
    sp, tp,
    q_ref, k_ref, v_ref, gate_ref, decay_ref, gain_ref, stream_ref,
    stream_all, gated_all,
    q_dec, out_acc, inc, dec, state_in, msg, got, gbuf,
    st_send, st_recv, sx_send, sx_recv, gx_send, gx_recv, loc_sem,
):
    me_sp, me_tp = lax.axis_index("sp"), lax.axis_index("tp")
    rows, key_w = q_ref.shape
    chunks = rows // CHUNK
    heads = key_w // HEAD_K
    own_rows = stream_ref.shape[0]
    val_w = v_ref.shape[1]

    barrier = pltpu.get_barrier_semaphore()
    for o in range(1, sp):
        pl.semaphore_signal(barrier, inc=1, device_id=(lax.rem(me_sp + o, sp), me_tp), device_id_type=MESH)
    for o in range(1, tp):
        pl.semaphore_signal(barrier, inc=1, device_id=(me_sp, lax.rem(me_tp + o, tp)), device_id_type=MESH)
    pl.semaphore_wait(barrier, sp + tp - 2)

    own_span = pl.ds(pl.multiple_of(me_tp * own_rows, own_rows), own_rows)
    stream_copies = []
    for o in range(1, tp):
        copy = pltpu.make_async_remote_copy(
            src_ref=stream_ref, dst_ref=stream_all.at[own_span, :],
            send_sem=sx_send.at[o - 1], recv_sem=sx_recv.at[o - 1],
            device_id=(me_sp, lax.rem(me_tp + o, tp)), device_id_type=MESH,
        )
        copy.start()
        stream_copies.append(copy)
    own_stream = pltpu.make_async_copy(stream_ref, stream_all.at[own_span, :], loc_sem.at[0])
    own_stream.start()

    row = lax.broadcasted_iota(jnp.int32, (CHUNK, CHUNK), 0)
    col = lax.broadcasted_iota(jnp.int32, (CHUNK, CHUNK), 1)
    lower = row >= col
    upper = row <= col
    tri = (lower.astype(f32).astype(bf16), upper.astype(f32).astype(bf16))
    ones = jnp.ones((2 * CHUNK, HEAD_V), bf16)
    lane = lax.broadcasted_iota(jnp.int32, (CHUNK, key_w), 1)
    head_mask = [(lane >= h * HEAD_K) & (lane < (h + 1) * HEAD_K) for h in range(heads)]
    zero = jnp.zeros((CHUNK, key_w), bf16)

    def first(c, carry):
        span = pl.ds(pl.multiple_of(c * CHUNK, CHUNK), CHUNK)
        q = q_ref[span, :].astype(f32) * HEAD_K ** (-0.5)
        k = k_ref[span, :].astype(f32)
        v = v_ref[span, :]
        scores = [None, None]
        for way in range(2):
            x = decay_ref[way, span, :]
            logd = (jnp.minimum(x, 0.0) - jnp.log1p(jnp.exp(-jnp.abs(x)))) * (1.0 / gate_temper)
            hi, lo = split_hi_lo(logd)
            within = dot(tri[way], hi) + dot(tri[way], lo)
            end = within[CHUNK - 1 : CHUNK, :] if way == 0 else within[0:1, :]
            qd = (q * jnp.exp(within)).astype(bf16)
            ki = (k * jnp.exp(-within)).astype(bf16)
            ke = (k * jnp.exp(end - within)).astype(bf16)
            q_dec[way, span, :] = qd
            scores[way] = [dot_t1(jnp.where(m, qd, zero), ki) for m in head_mask]
            full = dot_t0(ke, v)
            inc[way, c] = jnp.concatenate(
                [full[h * HEAD_K : (h + 1) * HEAD_K, h * HEAD_V : (h + 1) * HEAD_V] for h in range(heads)], axis=0
            )
            dec[way, c] = jnp.exp(dot_t0(jnp.concatenate([hi, lo], axis=0), ones))
        for h in range(heads):
            s = jnp.where(lower, scores[0][h], 0.0) + jnp.where(upper, scores[1][h], 0.0)
            out_acc[span, h * HEAD_V : (h + 1) * HEAD_V] = dot(s.astype(bf16), v[:, h * HEAD_V : (h + 1) * HEAD_V])
        return carry

    lax.fori_loop(0, chunks, first, 0)

    state_shape = (key_w, HEAD_V)
    for way in range(2):

        def total(i, carry):
            state, decay = carry
            c = i if way == 0 else chunks - 1 - i
            d = dec[way, c]
            return d * state + inc[way, c], d * decay

        state, decay = lax.fori_loop(0, chunks, total, (jnp.zeros(state_shape, f32), jnp.ones(state_shape, f32)))
        msg[way, 0:key_w, :] = state.astype(bf16)
        msg[way, key_w : 2 * key_w, :] = decay.astype(bf16)

    got[me_sp] = jnp.zeros(got.shape[1:], bf16)
    state_copies = []
    for o in range(1, sp):
        peer = lax.rem(me_sp + o, sp)
        way = jnp.where(peer > me_sp, 0, 1)
        copy = pltpu.make_async_remote_copy(
            src_ref=msg.at[way], dst_ref=got.at[me_sp],
            send_sem=st_send.at[o - 1], recv_sem=st_recv.at[o - 1],
            device_id=(peer, me_tp), device_id_type=MESH,
        )
        copy.start()
        state_copies.append(copy)
    for copy in state_copies:
        copy.wait()

    for way in range(2):

        def hop(i, state):
            at = i if way == 0 else sp - 1 - i
            reached = at < me_sp if way == 0 else at > me_sp
            block = got[at]
            new = block[key_w : 2 * key_w, :].astype(f32) * state + block[0:key_w, :].astype(f32)
            return jnp.where(reached, new, state)

        start = lax.fori_loop(0, sp, hop, jnp.zeros(state_shape, f32))

        def enter(i, state):
            c = i if way == 0 else chunks - 1 - i
            state_in[c, way * key_w : (way + 1) * key_w, :] = state.astype(bf16)
            return dec[way, c] * state + inc[way, c]

        lax.fori_loop(0, chunks, enter, start)

    def second(c, carry):
        span = pl.ds(pl.multiple_of(c * CHUNK, CHUNK), CHUNK)
        qf, qb = q_dec[0, span, :], q_dec[1, span, :]
        state = state_in[c]
        for h in range(heads):
            cols = slice(h * HEAD_V, (h + 1) * HEAD_V)
            m = head_mask[h]
            both = jnp.concatenate([jnp.where(m, qf, zero), jnp.where(m, qb, zero)], axis=1)
            att = out_acc[span, cols] + dot(both, state)
            inv = lax.rsqrt(jnp.mean(att * att, axis=-1, keepdims=True) + norm_eps)
            g = gate_ref[span, cols].astype(f32)
            silu = g / (1.0 + jnp.exp(-g))
            gbuf[span, cols] = (att * inv * gain_ref[0:1, cols] * silu).astype(bf16)
        return carry

    own_cols = pl.ds(pl.multiple_of(me_tp * val_w, val_w), val_w)
    gated_copies = []
    half = chunks // 2
    for part in range(2):
        lax.fori_loop(part * half, (part + 1) * half, second, 0)
        span = pl.ds(part * half * CHUNK, half * CHUNK)
        for o in range(1, tp):
            copy = pltpu.make_async_remote_copy(
                src_ref=gbuf.at[span, :], dst_ref=gated_all.at[span, own_cols],
                send_sem=gx_send.at[part, o - 1], recv_sem=gx_recv.at[part, o - 1],
                device_id=(me_sp, lax.rem(me_tp + o, tp)), device_id_type=MESH,
            )
            copy.start()
            gated_copies.append(copy)
    own_gated = pltpu.make_async_copy(gbuf, gated_all.at[:, own_cols], loc_sem.at[1])
    own_gated.start()
    for copy in stream_copies + gated_copies:
        copy.wait()
    own_stream.wait()
    own_gated.wait()


def attention(queries, keys, values, out_gate, decay_logit, head_gain, stream):
    sp, tp = lax.axis_size("sp"), lax.axis_size("tp")
    rows, key_w = queries.shape
    val_w = values.shape[1]
    chunks = rows // CHUNK
    own_rows, width = stream.shape
    vmem = pl.BlockSpec(memory_space=pltpu.VMEM)
    hbm = pl.BlockSpec(memory_space=pl.ANY)
    dma = pltpu.SemaphoreType.DMA
    return pl.pallas_call(
        functools.partial(attention_kernel, sp, tp),
        out_shape=(
            jax.ShapeDtypeStruct((own_rows * tp, width), bf16),
            jax.ShapeDtypeStruct((rows, val_w * tp), bf16),
        ),
        in_specs=[vmem] * 7,
        out_specs=(hbm, hbm),
        scratch_shapes=[
            pltpu.VMEM((2, rows, key_w), bf16),
            pltpu.VMEM((rows, val_w), f32),
            pltpu.VMEM((2, chunks, key_w, HEAD_V), f32),
            pltpu.VMEM((2, chunks, key_w, HEAD_V), f32),
            pltpu.VMEM((chunks, 2 * key_w, HEAD_V), bf16),
            pltpu.VMEM((2, 2 * key_w, HEAD_V), bf16),
            pltpu.VMEM((sp, 2 * key_w, HEAD_V), bf16),
            pltpu.VMEM((rows, val_w), bf16),
            dma((sp - 1,)), dma((sp - 1,)), dma((tp - 1,)), dma((tp - 1,)),
            dma((2, tp - 1)), dma((2, tp - 1)), dma((2,)),
        ],
        cost_estimate=pl.CostEstimate(flops=40_000_000_000, bytes_accessed=50_000_000, transcendentals=0),
        compiler_params=pltpu.CompilerParams(collective_id=0, has_side_effects=True),
        name="attention",
    )(queries, keys, values, out_gate, decay_logit, head_gain.reshape(1, val_w), stream)


def local(
    queries, keys, values, out_gate, decay_logit, head_gain, out_weight, stream, mlp_gain, up_weight, down_weight
):
    up_full = lax.all_gather(up_weight, "sp", axis=0, tiled=True)
    sp = lax.axis_size("sp")
    tp_index = lax.axis_index("tp")
    part_w = down_weight.shape[1] // 2
    down_parts = [
        lax.all_gather(down_weight[:, i * part_w : (i + 1) * part_w], "sp", axis=1, tiled=True) for i in range(2)
    ]
    stream_all, gated_all = attention(queries, keys, values, out_gate, decay_logit, head_gain, stream)
    own_rows = stream.shape[0]
    residual = (
        jnp.dot(gated_all, out_weight, preferred_element_type=f32) + stream_all.astype(f32)
    ).astype(bf16)
    wide = residual.astype(f32)
    normed = (wide * lax.rsqrt(jnp.mean(wide * wide, axis=-1, keepdims=True) + norm_eps) * mlp_gain).astype(bf16)
    hidden = jnp.square(jax.nn.relu(jnp.dot(normed, up_full, preferred_element_type=f32))).astype(bf16)
    hidden = lax.optimization_barrier(hidden)
    sums = [
        lax.psum_scatter(
            jnp.dot(hidden, part, preferred_element_type=f32).astype(bf16), "tp", scatter_dimension=0, tiled=True
        ).reshape(own_rows, sp, part_w)
        for part in down_parts
    ]
    mlp_sum = jnp.concatenate(sums, axis=2).reshape(own_rows, sp * 2 * part_w).astype(f32)
    own = lax.dynamic_slice_in_dim(residual, tp_index * own_rows, own_rows, 0)
    return (own.astype(f32) + mlp_sum).astype(bf16)


def solution(mesh):
    in_specs = (
        P("sp", "tp"), P("sp", "tp"), P("sp", "tp"), P("sp", "tp"), P(None, "sp", "tp"), P("tp"), P(),
        P(("sp", "tp"), None), P(), P("sp", "tp"), P("tp", "sp"),
    )
    return jax.shard_map(local, mesh=mesh, in_specs=in_specs, out_specs=P(("sp", "tp"), None), check_vma=False)
```

time: 705 us -> 374 us (0.53); the launches traced: 695 us -> 374 us
  other arithmetic: 146 us -> 2.68 us
  blocking collectives: 104 us -> 0 us
  Pallas kernels: 0 us -> 75.8 us
  local copies, waits for them, and re-layouts: 75.6 us -> 5.4 us
  waiting for transfers between devices: 290 us -> 234 us
  loops' own time: 12 us -> 0 us
  matrix products: 51.5 us -> 43.2 us
    all_gather x4 -> x0, blocking collectives: 104 us -> none  [carried_in(): lax.all_gather(part.astype(kind), axis)]
    another operation x8 -> x0, other arithmetic: 99.6 us -> none
    psum x1 -> x0, waiting for transfers between devices: 83.1 us -> none  [local(): summed = lax.psum((partial_value + placed).astype(jnp.bfloat16), 'tp')]
    pallas_call x0 -> x1, Pallas kernels: none -> 75.8 us  [attention(): pl.pallas_call(functools.partial(attention_kernel, sp, tp), out_shape=(ja...]
    dynamic_slice x32 -> x0, local copies, waits for them, and re-layouts: 22.7 us -> none  [blockwise(): lax.scan(advance, start_state, (jnp.exp(block_end), increments))]
    rev x5 -> x0, local copies, waits for them, and re-layouts: 21 us -> none  [the longest x1 9.35 us: local(): attended = fwd_out + jnp.flip(bwd_out, 0)]
    add x33 -> x0, other arithmetic: 16.8 us -> none  [the longest x32 16.3 us: advance(): return (decay_end[..., None] * carried + increment, carried)]
    all_gather x2 -> x3, waiting for transfers between devices: 163 us -> 177 us  [the longest x2 126 us: local(): lax.all_gather(down_weight[:, i * part_w:(i + 1) * part_w], 'sp', axis=1,...]
  transfers between devices with their start and end apart: 4 -> 5, of which waited for: 4 -> 5; matrix products, arithmetic and copies ran while one was open for 0% -> 12% of each run, Pallas kernels for 0% -> 20%
where the time goes in v1:
time: 374 us
  waiting for transfers between devices  234 us (63%)
  Pallas kernels  75.8 us (20%)
  matrix products  43.2 us (12%)
  between operations  13.2 us (4%)
  local copies, waits for them, and re-layouts  5.4 us (1%)
    all_gather x2, waiting for transfers between devices, local(): lax.all_gather(down_weight[:, i * part_w:(i + 1) * part_w], 'sp', axis=1,...  126 us
    pallas_call x1, Pallas kernels, attention(): pl.pallas_call(functools.partial(attention_kernel, sp, tp), out_shape=(ja...  75.8 us
    reduce_scatter x2, waiting for transfers between devices, local(): lax.psum_scatter(jnp.dot(hidden, part, preferred_element_type=f32).astype...  54.9 us
    all_gather x1, waiting for transfers between devices, local(): up_full = lax.all_gather(up_weight, 'sp', axis=0, tiled=True)  51 us
    dot_general x2, matrix products, local(): jnp.dot(hidden, part, preferred_element_type=f32).astype(bf16)  18.6 us
    dot_general x1, matrix products, local(): jnp.dot(normed, up_full, preferred_element_type=f32)  13.9 us
    dot_general x1, matrix products, local(): jnp.dot(gated_all, out_weight, preferred_element_type=f32)  10.7 us
  transfers between devices with their start and end apart: 5, of which 5 were waited for; matrix products, arithmetic and copies ran while one was open for 12% of the time, Pallas kernels for 20%

profile of v1, /device:TPU:0, one launch (start us, length us, event | category | flops | bytes accessed | tf_op | source)
XLA Modules:
  0.0 374.2 jit_solution(17400524489031541649)
XLA Ops:
  6.5 0.0 all-gather.4.cloned.1.call-start
  6.5 0.7 all-gather.4.cloned.1.call-update
  7.3 0.0 all-gather.6.cloned.1.call-start
  7.3 2.3 fusion.6
  9.6 0.0 all-gather.6.cloned.1.call-update
  9.6 0.0 all-gather.8.cloned.1.call-start
  9.6 0.7 all-gather.8.cloned.1.call-update
  10.3 0.0 reduce-scatter.3.cloned.1.call-start
  10.4 75.8 %attention.1 = (bf16[1024,2048]{1,0:T(8,128)(2,1)}, bf16[1024,1024]{1,0:T(8,128)(2,1)}) custom-call(bf16[1024,128]{1,0:T(8,128)(2,1)} %q_ref.1, bf16[1024,128]{1,0:T(8,128)(2,1)} %k_ref.1, bf16[1024,256]{1,0:T(8,128)(2,1)} %v_ref.1, bf16[1024,256]{1,0:T(8,128)(2,1)} %gate_ref.1, f32[2,1024,128]{2,1,0:T(8,128)} %decay_ref.1, f32[1,256]{1,0:T(1,128)} %bitcast.20, ...), custom_call_target="tpu_custom_call" | custom-call | flops 40000000000 | bytes 50000000 | tf_op jit(solution)/shard_map/attention/pallas_call | solution.py:201
  86.1 0.0 copy-start
  86.1 10.7 %fusion = (f32[1024]{0:T(1024)S(1)}, bf16[1024,2048]{1,0:T(8,128)(2,1)}) fusion(bf16[1024,2048]{1,0:T(8,128)(2,1)} %get-tuple-element.8, bf16[1024,1024]{1,0:T(8,128)(2,1)} %get-tuple-element.7, bf16[1024,2048]{1,0:T(8,128)(2,1)} %param.17), kind=kOutput, calls=%fused_computation.2 | convolution fusion | flops 4307549184 | bytes 14684160 | tf_op jit(solution)/shard_map/dot_general | solution.py:240
  96.9 51.0 %all-gather.4.cloned.1.call-done = bf16[2048,2048]{1,0:T(8,128)(2,1)} async-done(((bf16[256,2048]{1,0:T(8,128)(2,1)}), bf16[2048,2048]{1,0:T(8,128)(2,1)}) %all-gather.4.cloned.1.call-update) | async-done | bytes 8388624 | tf_op jit(solution)/shard_map/all_gather | solution.py:230
  147.8 0.0 copy-done
  147.8 13.9 %multiply_convert_fusion = bf16[1024,2048]{1,0:T(8,128)(2,1)} fusion(bf16[2048,2048]{1,0:T(8,128)(2,1)} %all-gather.4.cloned.1.call-done, bf16[1024,2048]{1,0:T(8,128)(2,1)} %get-tuple-element.12, f32[2048]{0:T(1024)S(1)} %copy-done, f32[1024]{0:T(1024)S(1)} %add_rsqrt_fusion), kind=kOutput, calls=%fused_computation.5 | convolution fusion | flops 8604614656 | bytes 16789504 | tf_op jit(solution)/shard_map/dot_general | solution.py:244
  161.7 61.0 %all-gather.6.cloned.1.call-done = bf16[2048,1024]{1,0:T(8,128)(2,1)} async-done(((bf16[2048,128]{1,0:T(8,128)(2,1)}), bf16[2048,1024]{1,0:T(8,128)(2,1)}) %all-gather.6.cloned.1.call-update) | async-done | bytes 4194320 | tf_op jit(solution)/shard_map/all_gather | solution.py:235
  222.7 9.3 %convolution_convert_fusion.1 = bf16[1024,1024]{1,0:T(8,128)(2,1)} fusion(bf16[1024,2048]{1,0:T(8,128)(2,1)} %multiply_convert_fusion, bf16[2048,1024]{1,0:T(8,128)(2,1)} %all-gather.6.cloned.1.call-done), kind=kOutput, calls=%fused_computation.11 | convolution fusion | flops 4296015872 | bytes 10485760 | tf_op jit(solution)/shard_map/dot_general | solution.py:248
  232.0 0.0 reduce-scatter.3.cloned.1.call-update
  232.0 0.2 reduce-scatter.5.cloned.1.call-start
  232.2 65.4 %all-gather.8.cloned.1.call-done = bf16[2048,1024]{1,0:T(8,128)(2,1)} async-done(((bf16[2048,128]{1,0:T(8,128)(2,1)}), bf16[2048,1024]{1,0:T(8,128)(2,1)}) %all-gather.8.cloned.1.call-update) | async-done | bytes 4194320 | tf_op jit(solution)/shard_map/all_gather | solution.py:235
  297.6 9.3 %convolution_convert_fusion = bf16[1024,1024]{1,0:T(8,128)(2,1)} fusion(bf16[1024,2048]{1,0:T(8,128)(2,1)} %multiply_convert_fusion, bf16[2048,1024]{1,0:T(8,128)(2,1)} %all-gather.8.cloned.1.call-done), kind=kOutput, calls=%fused_computation.10 | convolution fusion | flops 4296015872 | bytes 10485760 | tf_op jit(solution)/shard_map/dot_general | solution.py:248
  306.9 0.0 reduce-scatter.5.cloned.1.call-update
  306.9 22.5 %reduce-scatter.3.cloned.1.call-done = bf16[256,1024]{1,0:T(8,128)(2,1)} async-done(((bf16[1024,1024]{1,0:T(8,128)(2,1)}), bf16[256,1024]{1,0:T(8,128)(2,1)}) %reduce-scatter.3.cloned.1.call-update) | async-done | bytes 524304 | tf_op jit(solution)/shard_map/reduce_scatter | solution.py:247
  329.4 1.1 copy.12
  330.5 32.4 %reduce-scatter.5.cloned.1.call-done = bf16[256,1024]{1,0:T(8,128)(2,1)} async-done(((bf16[1024,1024]{1,0:T(8,128)(2,1)}), bf16[256,1024]{1,0:T(8,128)(2,1)}) %reduce-scatter.5.cloned.1.call-update) | async-done | bytes 524304 | tf_op jit(solution)/shard_map/reduce_scatter | solution.py:247
  363.0 1.1 copy.13
  364.1 0.1 maximum_convert_fusion
  364.2 0.9 copy.14
  365.1 2.5 add_convert_fusion.1
  (1 shorter events, 0.0 us)
Async XLA Ops:
  6.5 141.3 %all-gather.4.cloned.1.call-start = ((), (), s32[]{:S(2)}) async-start(), calls=%async_computation.2 | async-start | bytes 9437184 | tf_op jit(solution)/shard_map/all_gather | solution.py:230
  7.3 215.4 %all-gather.6.cloned.1.call-start = ((), (), s32[]{:S(2)}) async-start(), calls=%async_computation.3 | async-start | bytes 4718592 | tf_op jit(solution)/shard_map/all_gather | solution.py:235
  9.6 288.0 %all-gather.8.cloned.1.call-start = ((), (), s32[]{:S(2)}) async-start(), calls=%async_computation.5 | async-start | bytes 4718592 | tf_op jit(solution)/shard_map/all_gather | solution.py:235
  10.3 319.0 %reduce-scatter.3.cloned.1.call-start = ((), (), s32[]{:S(2)}) async-start(), calls=%async_computation.4 | async-start | bytes 2621440 | tf_op jit(solution)/shard_map/reduce_scatter | solution.py:247
  86.1 61.7 %copy-start = (f32[2048]{0:T(1024)S(1)}, f32[2048]{0:T(1024)}, u32[]{:S(2)}) copy-start(f32[2048]{0:T(1024)} %param.19) | copy-start | bytes 24580
  232.0 130.9 %reduce-scatter.5.cloned.1.call-start = ((), (), s32[]{:S(2)}) async-start(), calls=%async_computation.6 | async-start | bytes 2621440 | tf_op jit(solution)/shard_map/reduce_scatter | solution.py:247
Sparse Core Ops, SparseCore 0:
  9.5 138.3 all-gather.3
  149.8 72.7 all-gather.5
  224.7 72.8 all-gather.7
  300.0 29.3 reduce-scatter.2
  331.7 31.1 reduce-scatter.4

commit v2 on v1

--- a/solution.py
+++ b/solution.py
@@ -35,10 +35,10 @@
 
 def attention_kernel(
     sp, tp,
-    q_ref, k_ref, v_ref, gate_ref, decay_ref, gain_ref, stream_ref,
-    stream_all, gated_all,
+    q_ref, k_ref, v_ref, gate_ref, decay_ref, gain_ref, stream_ref, down_ref,
+    stream_all, gated_all, down_all,
     q_dec, out_acc, inc, dec, state_in, msg, got, gbuf,
-    st_send, st_recv, sx_send, sx_recv, gx_send, gx_recv, loc_sem,
+    st_send, st_recv, sx_send, sx_recv, gx_send, gx_recv, dn_send, dn_recv, loc_sem,
 ):
     me_sp, me_tp = lax.axis_index("sp"), lax.axis_index("tp")
     rows, key_w = q_ref.shape
@@ -54,6 +54,46 @@
         pl.semaphore_signal(barrier, inc=1, device_id=(me_sp, lax.rem(me_tp + o, tp)), device_id_type=MESH)
     pl.semaphore_wait(barrier, sp + tp - 2)
 
+    depth, part_w = down_ref.shape
+    steps = sp // 2
+
+    def ring_place(i):
+        return jnp.where(lax.rem(i, 2) == 0, i // 2, sp - 1 - i // 2)
+
+    def ring_device(p):
+        return jnp.where(p < steps, 2 * p, 2 * (sp - 1 - p) + 1)
+
+    place = ring_place(me_sp)
+
+    def ring_copies(step):
+        made = []
+        for way in range(2):
+            sign = 1 if way == 0 else -1
+            owner = ring_device(lax.rem(place - sign * (step - 1) + sp, sp))
+            peer = ring_device(lax.rem(place + sign + sp, sp))
+            span = pl.ds(way * (depth // 2), depth // 2) if step == steps else pl.ds(0, depth)
+            cols = pl.ds(pl.multiple_of(owner * part_w, part_w), part_w)
+            src = down_ref.at[span, :] if step == 1 else down_all.at[span, cols]
+            made.append(pltpu.make_async_remote_copy(
+                src_ref=src, dst_ref=down_all.at[span, cols],
+                send_sem=dn_send.at[way, step - 1], recv_sem=dn_recv.at[way, step - 1],
+                device_id=(peer, me_tp), device_id_type=MESH,
+            ))
+        return made
+
+    ring = [ring_copies(step) for step in range(1, steps + 1)]
+
+    def ring_start(step):
+        for way in range(2):
+            if step > 1:
+                ring[step - 2][way].wait_recv()
+            ring[step - 1][way].start()
+
+    ring_start(1)
+    own_down = pltpu.make_async_copy(
+        down_ref, down_all.at[:, pl.ds(pl.multiple_of(me_sp * part_w, part_w), part_w)], loc_sem.at[2]
+    )
+    own_down.start()
     own_span = pl.ds(pl.multiple_of(me_tp * own_rows, own_rows), own_rows)
     stream_copies = []
     for o in range(1, tp):
@@ -131,6 +171,8 @@
         )
         copy.start()
         state_copies.append(copy)
+    if steps > 1:
+        ring_start(2)
     for copy in state_copies:
         copy.wait()
 
@@ -183,13 +225,20 @@
             gated_copies.append(copy)
     own_gated = pltpu.make_async_copy(gbuf, gated_all.at[:, own_cols], loc_sem.at[1])
     own_gated.start()
+    for step in range(3, steps + 1):
+        ring_start(step)
+    for way in range(2):
+        for step in range(steps):
+            ring[step][way].wait_send()
+        ring[steps - 1][way].wait_recv()
+    own_down.wait()
     for copy in stream_copies + gated_copies:
         copy.wait()
     own_stream.wait()
     own_gated.wait()
 
 
-def attention(queries, keys, values, out_gate, decay_logit, head_gain, stream):
+def attention(queries, keys, values, out_gate, decay_logit, head_gain, stream, down_weight):
     sp, tp = lax.axis_size("sp"), lax.axis_size("tp")
     rows, key_w = queries.shape
     val_w = values.shape[1]
@@ -203,9 +252,10 @@
         out_shape=(
             jax.ShapeDtypeStruct((own_rows * tp, width), bf16),
             jax.ShapeDtypeStruct((rows, val_w * tp), bf16),
+            jax.ShapeDtypeStruct((down_weight.shape[0], down_weight.shape[1] * sp), bf16),
         ),
-        in_specs=[vmem] * 7,
-        out_specs=(hbm, hbm),
+        in_specs=[vmem] * 8,
+        out_specs=(hbm, hbm, hbm),
         scratch_shapes=[
             pltpu.VMEM((2, rows, key_w), bf16),
             pltpu.VMEM((rows, val_w), f32),
@@ -216,25 +266,23 @@
             pltpu.VMEM((sp, 2 * key_w, HEAD_V), bf16),
             pltpu.VMEM((rows, val_w), bf16),
             dma((sp - 1,)), dma((sp - 1,)), dma((tp - 1,)), dma((tp - 1,)),
-            dma((2, tp - 1)), dma((2, tp - 1)), dma((2,)),
+            dma((2, tp - 1)), dma((2, tp - 1)),
+            dma((2, sp // 2)), dma((2, sp // 2)), dma((3,)),
         ],
         cost_estimate=pl.CostEstimate(flops=40_000_000_000, bytes_accessed=50_000_000, transcendentals=0),
         compiler_params=pltpu.CompilerParams(collective_id=0, has_side_effects=True),
         name="attention",
-    )(queries, keys, values, out_gate, decay_logit, head_gain.reshape(1, val_w), stream)
+    )(queries, keys, values, out_gate, decay_logit, head_gain.reshape(1, val_w), stream, down_weight)
 
 
 def local(
     queries, keys, values, out_gate, decay_logit, head_gain, out_weight, stream, mlp_gain, up_weight, down_weight
 ):
     up_full = lax.all_gather(up_weight, "sp", axis=0, tiled=True)
-    sp = lax.axis_size("sp")
     tp_index = lax.axis_index("tp")
-    part_w = down_weight.shape[1] // 2
-    down_parts = [
-        lax.all_gather(down_weight[:, i * part_w : (i + 1) * part_w], "sp", axis=1, tiled=True) for i in range(2)
-    ]
-    stream_all, gated_all = attention(queries, keys, values, out_gate, decay_logit, head_gain, stream)
+    stream_all, gated_all, down_full = attention(
+        queries, keys, values, out_gate, decay_logit, head_gain, stream, down_weight
+    )
     own_rows = stream.shape[0]
     residual = (
         jnp.dot(gated_all, out_weight, preferred_element_type=f32) + stream_all.astype(f32)
@@ -242,14 +290,9 @@
     wide = residual.astype(f32)
     normed = (wide * lax.rsqrt(jnp.mean(wide * wide, axis=-1, keepdims=True) + norm_eps) * mlp_gain).astype(bf16)
     hidden = jnp.square(jax.nn.relu(jnp.dot(normed, up_full, preferred_element_type=f32))).astype(bf16)
-    hidden = lax.optimization_barrier(hidden)
-    sums = [
-        lax.psum_scatter(
-            jnp.dot(hidden, part, preferred_element_type=f32).astype(bf16), "tp", scatter_dimension=0, tiled=True
-        ).reshape(own_rows, sp, part_w)
-        for part in down_parts
-    ]
-    mlp_sum = jnp.concatenate(sums, axis=2).reshape(own_rows, sp * 2 * part_w).astype(f32)
+    mlp_sum = lax.psum_scatter(
+        jnp.dot(hidden, down_full, preferred_element_type=f32).astype(bf16), "tp", scatter_dimension=0, tiled=True
+    ).astype(f32)
     own = lax.dynamic_slice_in_dim(residual, tp_index * own_rows, own_rows, 0)
     return (own.astype(f32) + mlp_sum).astype(bf16)
 

time: 374 us -> 297 us (0.79)
  waiting for transfers between devices: 234 us -> 46.1 us
  Pallas kernels: 75.8 us -> 199 us
  matrix products: 43.2 us -> 36.3 us
  local copies, waits for them, and re-layouts: 5.4 us -> 0.01 us
    all_gather x2 -> x0, waiting for transfers between devices: 126 us -> none  [local(): lax.all_gather(down_weight[:, i * part_w:(i + 1) * part_w], 'sp', axis=1,...]
    pallas_call x1, Pallas kernels: 75.8 us -> 199 us  [attention(): pl.pallas_call(functools.partial(attention_kernel, sp, tp), out_shape=(ja...]
    all_gather x1, waiting for transfers between devices: 51 us -> 0.01 us  [local(): up_full = lax.all_gather(up_weight, 'sp', axis=0, tiled=True)]
    reduce_scatter x2 -> x1, waiting for transfers between devices: 54.9 us -> 45.4 us  [local(): lax.psum_scatter(jnp.dot(hidden, down_full, preferred_element_type=f32).a...]
    dot_general x3 -> x1, matrix products: 32.5 us -> 25.7 us  [local(): jnp.dot(hidden, down_full, preferred_element_type=f32).astype(bf16)]
  transfers between devices with their start and end apart: 5 -> 2, of which waited for: 5 -> 1; matrix products, arithmetic and copies ran while one was open for 12% -> 4% of each run, Pallas kernels for 20% -> 67%
where the time goes in v2:
time: 297 us
  Pallas kernels  199 us (67%)
  waiting for transfers between devices  46.1 us (16%)
  matrix products  36.3 us (12%)
  between operations  13.4 us (5%)
    pallas_call x1, Pallas kernels, attention(): pl.pallas_call(functools.partial(attention_kernel, sp, tp), out_shape=(ja...  199 us
    reduce_scatter x1, waiting for transfers between devices, local(): lax.psum_scatter(jnp.dot(hidden, down_full, preferred_element_type=f32).a...  45.4 us
    dot_general x1, matrix products, local(): jnp.dot(hidden, down_full, preferred_element_type=f32).astype(bf16)  25.7 us
    dot_general x1, matrix products, local(): jnp.dot(gated_all, out_weight, preferred_element_type=f32)  10.7 us
  transfers between devices with their start and end apart: 2, of which 1 were waited for; matrix products, arithmetic and copies ran while one was open for 4% of the time, Pallas kernels for 67%

profile of v2, /device:TPU:0, one launch (start us, length us, event | category | flops | bytes accessed | tf_op | source)
XLA Modules:
  0.0 297.3 jit_solution(16891975705414300407)
XLA Ops:
  6.5 0.0 all-gather.2.cloned.1.call-start
  6.5 0.7 all-gather.2.cloned.1.call-update
  7.3 0.0 reduce-scatter.2.cloned.1.call-start
  7.3 198.5 %attention.1 = (bf16[1024,2048]{1,0:T(8,128)(2,1)}, bf16[1024,1024]{1,0:T(8,128)(2,1)}, bf16[2048,2048]{1,0:T(8,128)(2,1)}) custom-call(bf16[1024,128]{1,0:T(8,128)(2,1)} %q_ref.1, bf16[1024,128]{1,0:T(8,128)(2,1)} %k_ref.1, bf16[1024,256]{1,0:T(8,128)(2,1)} %v_ref.1, bf16[1024,256]{1,0:T(8,128)(2,1)} %gate_ref.1, f32[2,1024,128]{2,1,0:T(8,128)} %decay_ref.1, ...), custom_call_target="tpu_custom_call" | custom-call | flops 40000000000 | bytes 50000000 | tf_op jit(solution)/shard_map/attention/pallas_call | solution.py:250
  205.8 0.0 copy-start
  205.8 10.7 %fusion = (f32[1024]{0:T(1024)S(1)}, bf16[1024,2048]{1,0:T(8,128)(2,1)}) fusion(bf16[1024,2048]{1,0:T(8,128)(2,1)} %get-tuple-element.9, bf16[1024,1024]{1,0:T(8,128)(2,1)} %get-tuple-element.8, bf16[1024,2048]{1,0:T(8,128)(2,1)} %param.17), kind=kOutput, calls=%fused_computation.2 | convolution fusion | flops 4307549184 | bytes 14684160 | tf_op jit(solution)/shard_map/dot_general | solution.py:288
  216.5 0.0 all-gather.2.cloned.1.call-done
  216.5 0.0 copy-done
  216.5 25.7 %fusion.12 = bf16[1024,2048]{1,0:T(8,128)(2,1)} fusion(bf16[2048,2048]{1,0:T(8,128)(2,1)} %get-tuple-element.10, bf16[2048,2048]{1,0:T(8,128)(2,1)} %all-gather.2.cloned.1.call-done, bf16[1024,2048]{1,0:T(8,128)(2,1)} %get-tuple-element.12, f32[2048]{0:T(1024)S(1)} %copy-done, f32[1024]{0:T(1024)S(1)} %add_rsqrt_fusion), kind=kOutput, calls=%fused_computation.11 | convolution fusion | flops 17196646400 | bytes 25178112 | tf_op jit(solution)/shard_map/dot_general | solution.py:294
  242.2 0.0 reduce-scatter.2.cloned.1.call-update
  242.2 45.4 %reduce-scatter.2.cloned.1.call-done = bf16[256,2048]{1,0:T(8,128)(2,1)} async-done(((bf16[1024,2048]{1,0:T(8,128)(2,1)}), bf16[256,2048]{1,0:T(8,128)(2,1)}) %reduce-scatter.2.cloned.1.call-update) | async-done | bytes 1048592 | tf_op jit(solution)/shard_map/reduce_scatter | solution.py:293
  287.6 2.9 add_convert_fusion.1
  (1 shorter events, 0.0 us)
Async XLA Ops:
  6.5 210.0 %all-gather.2.cloned.1.call-start = ((), (), s32[]{:S(2)}) async-start(), calls=%async_computation.1 | async-start | bytes 9437184 | tf_op jit(solution)/shard_map/all_gather | solution.py:281
  7.3 280.3 %reduce-scatter.2.cloned.1.call-start = ((), (), s32[]{:S(2)}) async-start(), calls=%async_computation.2 | async-start | bytes 5242880 | tf_op jit(solution)/shard_map/reduce_scatter | solution.py:293
  205.8 10.7 %copy-start = (f32[2048]{0:T(1024)S(1)}, f32[2048]{0:T(1024)}, u32[]{:S(2)}) copy-start(f32[2048]{0:T(1024)} %param.19) | copy-start | bytes 24580
Sparse Core Ops, SparseCore 0:
  9.5 194.6 all-gather.1
  242.3 45.2 reduce-scatter.1
